TPU v7x, 128 devices: a whole 4x4x4 slice. The times are simulated.
128 devices in a mesh: ep: 128 (over z, y, x, core).
Axes of the slice: x: 4, y: 4, z: 4, core: 2. Of those that a mesh axis runs over, the one named last changes fastest.
Arguments:
- hidden_in: bfloat16 [256, 2048], P('ep'), may hold values from -6 to 6
- lengths: int32 [256], P('ep'), may hold values from 1 to 1024, as said below
- key_cache: bfloat16 [256, 1024, 512], P('ep'), may hold values from -30 to 30
- value_cache: bfloat16 [256, 1024, 512], P('ep'), may hold values from -6 to 6
- query_w: bfloat16 [2048, 2048], P('ep'), may hold values from -0.125 to 0.125
- key_w: bfloat16 [2048, 512], P('ep'), may hold values from -0.125 to 0.125
- value_w: bfloat16 [2048, 512], P('ep'), may hold values from -0.125 to 0.125
- out_w: bfloat16 [2048, 2048], P('ep'), may hold values from -0.125 to 0.125
- lam_heads: float32 [8], replicated, may hold values from 0.3 to 0.8
- head_gain: float32 [256], replicated, may hold values from 0.1 to 1.9
- attn_gain: float32 [2048], replicated, may hold values from 0.1 to 1.9
- moe_gain: float32 [2048], replicated, may hold values from 0.1 to 1.9
- routing: int32 [256, 6], replicated, may hold values from 0 to 127, all different within a row; in each aligned block of 256 rows (0 to 255, 256 to 511, ...) at most 24 rows name the same one
- route_weight: float32 [256, 6], replicated, may hold values from 0.1 to 0.6
- gate_w: bfloat16 [128, 2048, 512], P('ep'), may hold values from -0.125 to 0.125
- up_w: bfloat16 [128, 2048, 512], P('ep'), may hold values from -0.125 to 0.125
- down_w: bfloat16 [128, 512, 2048], P('ep'), may hold values from -0.25 to 0.25
- shared_gate: bfloat16 [2048, 512], replicated, may hold values from -0.125 to 0.125
- shared_up: bfloat16 [2048, 512], replicated, may hold values from -0.125 to 0.125
- shared_down: bfloat16 [512, 2048], replicated, may hold values from -0.25 to 0.25
Outputs:
- layer_out: bfloat16 [256, 2048], P('ep')
- key_new: bfloat16 [256, 512], P('ep')
- value_new: bfloat16 [256, 512], P('ep')
Inputs may be any that keep to these rules, and one draw needn't show every extreme that they name: `lengths`: some sequence has exactly 1024 positions in use. `routing`: each row names 6 different experts; no expert is named by more than 24 rows, a bound that some block reaches.
All inputs are finite; a program needn't handle non-finite values.
Results may differ from a plain program's by a relative error of at most 0.013.
The roundings to bfloat16 on the way count: a program that leaves them out, or rounds other values in their place, can miss the bound.
Values may be sent and summed in bfloat16 or wider, within the bound.
No kernel may reach another device: no remote copies, remote signals or barrier semaphores. Data moves between devices by JAX's collectives and lax.ppermute only.
A program may use at most 64 MiB of HBM per device.

v0:
```python
import jax
import jax.numpy as jnp
from jax import lax
from jax.sharding import Mesh
from jax.sharding import PartitionSpec as P

KV_HEADS = 2
HEAD_DIM = 128
EXP_CAP = 24
EP = ("ep_0", "ep_1", "ep_2", "ep_3")


eps_norm = 1e-06
eps_head = 1e-05
theta_base = 500000.0


def split_up(value, dim, length):
    dims = value.shape
    blocks = value.reshape(*dims[:dim], length, dims[dim] // length, *dims[dim + 1 :])
    return jnp.moveaxis(blocks, dim, 0)


def sent_and_summed(value, axis, dim):
    blocks = split_up(value, dim, lax.axis_size(axis))
    arrived = lax.all_to_all(blocks, axis, split_axis=0, concat_axis=0, tiled=True)
    return arrived.astype(jnp.float32).sum(axis=0)


def summed_rows(value, axes, dim):
    far, near = axes
    blocks = split_up(value, dim, lax.axis_size(far))
    nearer = sent_and_summed(blocks, near, dim + 1)
    arrived = lax.all_to_all(
        nearer.astype(jnp.bfloat16), far, split_axis=0, concat_axis=0, tiled=True
    )
    return arrived.astype(jnp.float32).sum(axis=0)


def rms_scale(row_block, gain_vec, epsilon):
    row_block = row_block.astype(jnp.float32)
    return (
        row_block
        * lax.rsqrt(jnp.mean(row_block * row_block, axis=-1, keepdims=True) + epsilon)
        * gain_vec
    )


def rotate(vectors, positions):
    half_width = vectors.shape[-1] // 2
    inverse = theta_base ** (-jnp.arange(half_width, dtype=jnp.float32) / half_width)
    angles = positions.astype(jnp.float32)[..., None] * inverse
    cosine, sine_part = (jnp.cos(angles), jnp.sin(angles))
    lower_half, upper_half = (vectors[..., :half_width], vectors[..., half_width:])
    return jnp.concatenate(
        [
            lower_half * cosine - upper_half * sine_part,
            lower_half * sine_part + upper_half * cosine,
        ],
        axis=-1,
    )


def attend(queries, key_new, value_new, cache_keys, cache_values, lengths, lam_heads, head_gain):
    num_seqs, kv_heads, group_size = (queries.shape[0], queries.shape[1], queries.shape[2])
    head_dim = queries.shape[-1]
    cache_len = cache_keys.shape[1]
    cache_keys = cache_keys.reshape(num_seqs, cache_len, kv_heads, 2, head_dim)
    cache_values = cache_values.reshape(num_seqs, cache_len, kv_heads, -1)
    value_new = value_new.reshape(num_seqs, kv_heads, -1)
    score_scale = head_dim ** (-0.5)
    scores = (
        jnp.einsum("skgph,sckph->skgpc", queries, cache_keys, preferred_element_type=jnp.float32)
        * score_scale
    )
    self_score = (
        jnp.einsum("skgph,skph->skgp", queries, key_new, preferred_element_type=jnp.float32)
        * score_scale
    )
    live_mask = (jnp.arange(cache_len)[None, :] < lengths[:, None])[:, None, None, None, :]
    peak = jnp.maximum(jnp.max(jnp.where(live_mask, scores, -jnp.inf), axis=-1), self_score)
    weights = jnp.where(live_mask, jnp.exp(scores - peak[..., None]), 0.0)
    self_weight = jnp.exp(self_score - peak)
    totals = jnp.sum(weights, axis=-1) + self_weight
    lambda_grid = lam_heads.reshape(kv_heads, group_size)[None]
    combined = (
        weights[:, :, :, 0] / totals[:, :, :, 0, None]
        - lambda_grid[..., None] * weights[:, :, :, 1] / totals[:, :, :, 1, None]
    ).astype(jnp.bfloat16)
    self_combined = (
        self_weight[..., 0] / totals[..., 0] - lambda_grid * self_weight[..., 1] / totals[..., 1]
    ).astype(jnp.bfloat16)
    head_out = jnp.einsum(
        "skgc,sckv->skgv", combined, cache_values, preferred_element_type=jnp.float32
    )
    head_out = (
        head_out
        + self_combined.astype(jnp.float32)[..., None]
        * value_new.astype(jnp.float32)[:, :, None, :]
    )
    return rms_scale(head_out, head_gain, eps_head).astype(jnp.bfloat16).reshape(num_seqs, -1)


def expert_rows(row_block, routed_here, gate_one, up_one, down_one):
    slot_index = jnp.cumsum(routed_here) - 1
    pick_table = (
        (slot_index[None, :] == jnp.arange(EXP_CAP)[:, None]) & (routed_here[None, :] > 0)
    ).astype(jnp.bfloat16)
    picked = jnp.dot(pick_table, row_block, preferred_element_type=jnp.float32).astype(jnp.bfloat16)
    hidden = (
        jax.nn.silu(jnp.dot(picked, gate_one, preferred_element_type=jnp.float32))
        * jnp.dot(picked, up_one, preferred_element_type=jnp.float32)
    ).astype(jnp.bfloat16)
    result = jnp.dot(hidden, down_one, preferred_element_type=jnp.float32).astype(jnp.bfloat16)
    return jnp.dot(pick_table.T, result, preferred_element_type=jnp.float32)


def on_device(
    hidden_in,
    lengths,
    key_cache,
    value_cache,
    query_w,
    key_w,
    value_w,
    out_w,
    lam_heads,
    head_gain,
    attn_gain,
    moe_gain,
    routing,
    route_weight,
    gate_w,
    up_w,
    down_w,
    shared_gate,
    shared_up,
    shared_down,
):
    devices = lax.axis_size(EP)
    device = lax.axis_index(EP)
    tok_dev = hidden_in.shape[0]
    model_width = hidden_in.shape[1]
    all_rows = lax.all_gather(hidden_in, EP, axis=0, tiled=True)
    normed = rms_scale(all_rows, attn_gain, eps_norm).astype(jnp.bfloat16)
    joined_rows = jnp.concatenate([query_w, key_w, value_w], axis=1)
    column_block = lax.all_to_all(joined_rows, EP, split_axis=1, concat_axis=0, tiled=True)
    column_sums = jnp.dot(normed, column_block, preferred_element_type=jnp.float32)
    projected = lax.all_to_all(column_sums, EP, split_axis=0, concat_axis=1, tiled=True)
    query_cols = query_w.shape[1]
    key_cols = key_w.shape[1]
    queries = rotate(
        projected[:, :query_cols].reshape(tok_dev, KV_HEADS, -1, 2, HEAD_DIM),
        lengths[:, None, None, None],
    ).astype(jnp.bfloat16)
    key_new = rotate(
        projected[:, query_cols : query_cols + key_cols].reshape(tok_dev, KV_HEADS, 2, HEAD_DIM),
        lengths[:, None, None],
    ).astype(jnp.bfloat16)
    value_new = projected[:, query_cols + key_cols :].astype(jnp.bfloat16)
    attn_out = attend(
        queries, key_new, value_new, key_cache, value_cache, lengths, lam_heads, head_gain
    )
    pieces = lax.all_to_all(attn_out, EP, split_axis=1, concat_axis=0, tiled=True)
    routed_here = jnp.sum((routing == device).astype(jnp.int32), axis=1)
    attn_proj = summed_rows(
        jnp.dot(pieces, out_w, preferred_element_type=jnp.float32).astype(jnp.bfloat16),
        (("ep_0", "ep_1", "ep_2"), "ep_3"),
        0,
    ).astype(jnp.bfloat16)
    after_mixer = (hidden_in.astype(jnp.float32) + attn_proj.astype(jnp.float32)).astype(
        jnp.bfloat16
    )
    moe_in = rms_scale(after_mixer, moe_gain, eps_norm).astype(jnp.bfloat16)
    own_routes = lax.dynamic_slice_in_dim(routing, device * tok_dev, tok_dev, 0)
    own_weights = lax.dynamic_slice_in_dim(route_weight, device * tok_dev, tok_dev, 0)
    expert_ids = jnp.arange(devices, dtype=jnp.int32)
    matches = own_routes[:, :, None] == expert_ids[None, None, :]
    chosen = jnp.any(matches, axis=1)
    weight_grid = jnp.sum(jnp.where(matches, own_weights[:, :, None], 0.0), axis=1)
    outgoing = jnp.where(chosen.T[:, :, None], moe_in[None], jnp.zeros((), jnp.bfloat16))
    arrived = lax.all_to_all(outgoing, EP, split_axis=0, concat_axis=0, tiled=True)
    result = expert_rows(
        arrived.reshape(devices * tok_dev, model_width), routed_here, gate_w[0], up_w[0], down_w[0]
    ).astype(jnp.bfloat16)
    returned = lax.all_to_all(
        result.reshape(devices, tok_dev, model_width), EP, split_axis=0, concat_axis=0, tiled=True
    )
    routed = jnp.sum(returned.astype(jnp.float32) * weight_grid.T[:, :, None], axis=0)
    shared_hidden = (
        jax.nn.silu(jnp.dot(moe_in, shared_gate, preferred_element_type=jnp.float32))
        * jnp.dot(moe_in, shared_up, preferred_element_type=jnp.float32)
    ).astype(jnp.bfloat16)
    shared_out = jnp.dot(shared_hidden, shared_down, preferred_element_type=jnp.float32)
    layer_out = (after_mixer.astype(jnp.float32) + routed + shared_out).astype(jnp.bfloat16)
    return (layer_out, key_new.reshape(tok_dev, -1), value_new)


def solution(mesh):
    torus = Mesh(mesh.devices.reshape(4, 4, 4, 2), ("ep_0", "ep_1", "ep_2", "ep_3"))
    return jax.shard_map(
        on_device,
        mesh=torus,
        in_specs=(
            P(EP, None),
            P(EP),
            P(EP, None, None),
            P(EP, None, None),
            P(EP, None),
            P(EP, None),
            P(EP, None),
            P(EP, None),
            P(),
            P(),
            P(),
            P(),
            P(),
            P(),
            P(EP, None, None),
            P(EP, None, None),
            P(EP, None, None),
            P(),
            P(),
            P(),
        ),
        out_specs=(P(EP, None), P(EP, None), P(EP, None)),
        check_vma=False,
    )
```

profile of v0, /device:TPU:1, one launch (start us, length us, event | category | flops | bytes accessed | tf_op | source)
XLA Modules:
  0.0 221.3 jit_solution(17257553948698546519)
XLA Ops:
  11.2 11.5 %all-to-all-start = ((bf16[128,2,192]{2,1,0:T(2,128)(2,1)}), bf16[128,2,192]{2,1,0:T(2,128)(2,1)S(1)}, u32[]{:S(2)}, u32[]{:S(2)}) async-start(bf16[128,2,192]{2,1,0:T(2,128)(2,1)} %reshape.270), calls=%async_computation | async-start | bytes 262144 | tf_op jit(solution)/shard_map/all_to_all | solution.py:147
  22.8 9.9 %all-to-all-done = bf16[128,2,192]{2,1,0:T(2,128)(2,1)S(1)} async-done(((bf16[128,2,192]{2,1,0:T(2,128)(2,1)}), bf16[128,2,192]{2,1,0:T(2,128)(2,1)S(1)}, u32[]{:S(2)}, u32[]{:S(2)}) %all-to-all-start) | async-done | bytes 98336 | tf_op jit(solution)/shard_map/all_to_all | solution.py:147
  33.9 44.1 %all-gather.3.cloned.1.call-done = bf16[128,2,2048]{2,1,0:T(2,128)(2,1)} async-done(((bf16[1,2,2048]{2,1,0:T(2,128)(2,1)}), bf16[128,2,2048]{2,1,0:T(2,128)(2,1)}) %all-gather.3.cloned.1.call-update) | async-done | bytes 1048592 | tf_op jit(solution)/shard_map/all_gather | solution.py:144
  78.0 2.5 %reshape.265 = f32[256,2048]{1,0:T(8,128)} reshape(bf16[128,2,2048]{2,1,0:T(2,128)(2,1)} %all-gather.3.cloned.1.call-done) | data formatting | bytes 3145728 | tf_op jit(solution)/shard_map/convert_element_type | solution.py:41
  80.6 2.0 multiply_reduce_fusion.1
  84.5 2.1 fusion.29
  87.4 5.4 %all-to-all-start.1 = ((f32[128,2,24]{2,1,0:T(2,128)}), f32[128,2,24]{2,1,0:T(2,128)S(1)}, u32[]{:S(2)}, u32[]{:S(2)}) async-start(f32[128,2,24]{2,1,0:T(2,128)} %copy.77), calls=%async_computation.1 | async-start | bytes 262144 | tf_op jit(solution)/shard_map/all_to_all | solution.py:149
  92.9 4.0 %reshape.254 = bf16[2,1024,2,2,128]{4,3,2,1,0:T(2,128)(2,1)} reshape(bf16[2,1024,512]{2,1,0:T(8,128)(2,1)} %param.22) | data formatting | bytes 4194304 | tf_op jit(solution)/shard_map/reshape | solution.py:68
  96.9 5.8 %all-to-all-done.1 = f32[128,2,24]{2,1,0:T(2,128)S(1)} async-done(((f32[128,2,24]{2,1,0:T(2,128)}), f32[128,2,24]{2,1,0:T(2,128)S(1)}, u32[]{:S(2)}, u32[]{:S(2)}) %all-to-all-start.1) | async-done | bytes 24608 | tf_op jit(solution)/shard_map/all_to_all | solution.py:149
  103.5 2.4 %select_reduce_fusion = (f32[2,2,4,2]{2,3,1,0:T(2,128)S(1)}, f32[2,2,4,2,1024]{4,2,3,1,0:T(4,128)S(1)}) fusion(pred[2,1024]{1,0:T(4,128)(4,1)S(1)} %iota_compare_fusion.1, bf16[2,1024,2,2,128]{4,3,2,1,0:T(2,128)(2,1)} %reshape.254, bf16[2,2,4,2,64]{4,2,3,1,0:T(4,128)(2,1)S(1)} %get-tuple-element.8, bf16[2,2,4,2,64]{4,2,3,1,0:T(4,128)(2,1)S(1)} %get-tuple-element.7), kind=kOutput, calls=%fused_computation.31 | convolution fusion | flops 8503264 | bytes 2238592 | tf_op jit(solution)/shard_map/skgph,sckph->skgpc/dot_general | solution.py:73
  106.1 2.1 multiply_reduce_fusion.2
  108.5 13.7 %all_to_all.74 = bf16[2,128,16]{2,0,1:T(2,128)(2,1)S(1)} all-to-all(bf16[2,128,16]{2,0,1:T(2,128)(2,1)S(1)} %copy.84), channel_id=1, replica_groups=mesh['ep_0'=4,'ep_1'=4,'ep_2'=4,'ep_3'=2] {'ep_0','ep_1','ep_2','ep_3'}, dimensions={1} | all-to-all | bytes 16384 | tf_op jit(solution)/shard_map/all_to_all | solution.py:164
  124.1 1.9 copy.125
  126.0 5.0 %all_to_all.75 = bf16[2,64,2,2048]{3,2,1,0:T(2,128)(2,1)S(1)} all-to-all(bf16[2,64,2,2048]{3,2,1,0:T(2,128)(2,1)S(1)} %bitcast.97), channel_id=1, replica_groups=mesh['ep_0'=4,'ep_1'=4,'ep_2'=4,'ep_3'=2] {'ep_3'}, dimensions={0} | all-to-all | bytes 2097152 | tf_op jit(solution)/shard_map/all_to_all | solution.py:26
  131.0 3.1 %reduce_sum.90 = bf16[64,2,2048]{2,1,0:T(2,128)(2,1)} reduce(bf16[2,64,2,2048]{3,2,1,0:T(2,128)(2,1)S(1)} %all_to_all.75, bf16[]{:T(256)} %constant.30.clone.1), dimensions={0}, to_apply=%region_4.5 | reduce | flops 262144 | bytes 1572866 | tf_op jit(solution)/shard_map/reduce_sum | solution.py:27
  134.1 4.9 %all-to-all-start.4 = ((bf16[64,2,2048]{2,1,0:T(2,128)(2,1)}), bf16[64,2,2048]{2,1,0:T(2,128)(2,1)S(1)}, u32[]{:S(2)}, u32[]{:S(2)}) async-start(bf16[64,2,2048]{2,1,0:T(2,128)(2,1)} %reduce_sum.90), calls=%async_computation.4 | async-start | bytes 1048576 | tf_op jit(solution)/shard_map/all_to_all | solution.py:34
  139.3 12.1 %all-to-all-done.4 = bf16[64,2,2048]{2,1,0:T(2,128)(2,1)S(1)} async-done(((bf16[64,2,2048]{2,1,0:T(2,128)(2,1)}), bf16[64,2,2048]{2,1,0:T(2,128)(2,1)S(1)}, u32[]{:S(2)}, u32[]{:S(2)}) %all-to-all-start.4) | async-done | bytes 524320 | tf_op jit(solution)/shard_map/all_to_all | solution.py:34
  153.9 5.3 %all-to-all-start.5 = ((bf16[128,2,2048]{2,1,0:T(2,128)(2,1)}), bf16[128,2,2048]{2,1,0:T(2,128)(2,1)S(1)}, u32[]{:S(2)}, u32[]{:S(2)}) async-start(bf16[128,2,2048]{2,1,0:T(2,128)(2,1)} %broadcast_select_fusion), calls=%async_computation.5 | async-start | bytes 2097152 | tf_op jit(solution)/shard_map/all_to_all | solution.py:182
  159.8 18.7 %all-to-all-done.5 = bf16[128,2,2048]{2,1,0:T(2,128)(2,1)S(1)} async-done(((bf16[128,2,2048]{2,1,0:T(2,128)(2,1)}), bf16[128,2,2048]{2,1,0:T(2,128)(2,1)S(1)}, u32[]{:S(2)}, u32[]{:S(2)}) %all-to-all-start.5) | async-done | bytes 1048608 | tf_op jit(solution)/shard_map/all_to_all | solution.py:182
  181.4 2.0 fusion.7
  186.0 4.4 %all-to-all-start.6 = ((bf16[128,2,2048]{2,1,0:T(2,128)(2,1)}), bf16[128,2,2048]{2,1,0:T(2,128)(2,1)S(1)}, u32[]{:S(2)}, u32[]{:S(2)}) async-start(bf16[128,2,2048]{2,1,0:T(2,128)(2,1)} %reshape.260), calls=%async_computation.6 | async-start | bytes 2097152 | tf_op jit(solution)/shard_map/all_to_all | solution.py:186
  191.4 2.0 fusion.62
  193.4 16.4 %all-to-all-done.6 = bf16[128,2,2048]{2,1,0:T(2,128)(2,1)S(1)} async-done(((bf16[128,2,2048]{2,1,0:T(2,128)(2,1)}), bf16[128,2,2048]{2,1,0:T(2,128)(2,1)S(1)}, u32[]{:S(2)}, u32[]{:S(2)}) %all-to-all-start.6) | async-done | bytes 1048608 | tf_op jit(solution)/shard_map/all_to_all | solution.py:186
  210.9 3.6 %fusion = bf16[2,2048]{1,0:T(2,128)(2,1)} fusion(bf16[512,2048]{1,0:T(8,128)(2,1)} %param.39, bf16[2,2048]{1,0:T(2,128)(2,1)S(1)} %fusion.42, bf16[2048,512]{1,0:T(8,128)(2,1)} %param.38, f32[2,2048]{1,0:T(2,128)S(1)} %multiply_reduce_fusion, f32[2,512]{1,0:T(2,128)S(1)} %fusion.62, bf16[2,2048]{1,0:T(2,128)(2,1)S(1)} %reduce_sum.91, ...), kind=kOutput, calls=%fused_computation.5 | convolution fusion | flops 8427520 | bytes 4247552 | tf_op jit(solution)/shard_map/dot_general | solution.py:194
  (91 shorter events, 22.3 us)
Async XLA Ops:
  7.2 176.6 %copy-start = (bf16[1,512,2048]{2,1,0:T(8,128)(2,1)S(1)}, bf16[1,512,2048]{2,1,0:T(8,128)(2,1)}, u32[]{:S(2)}) copy-start(bf16[1,512,2048]{2,1,0:T(8,128)(2,1)} %param.36) | copy-start | bytes 6291460
  7.2 15.5 %copy-start.11 = (s32[2]{0:T(128)S(1)}, s32[2]{0:T(128)}, u32[]{:S(2)}) copy-start(s32[2]{0:T(128)} %param.21) | copy-start | bytes 28
  7.2 70.8 %all-gather.3.cloned.1.call-start = ((), (), s32[]{:S(2)}) async-start(), calls=%async_computation.7 | async-start | bytes 1056768 | tf_op jit(solution)/shard_map/all_gather | solution.py:144
  11.2 21.5 %all-to-all-start = ((bf16[128,2,192]{2,1,0:T(2,128)(2,1)}), bf16[128,2,192]{2,1,0:T(2,128)(2,1)S(1)}, u32[]{:S(2)}, u32[]{:S(2)}) async-start(bf16[128,2,192]{2,1,0:T(2,128)(2,1)} %reshape.270), calls=%async_computation | async-start | bytes 262144 | tf_op jit(solution)/shard_map/all_to_all | solution.py:147
  33.9 48.7 %copy-start.6 = (f32[2048]{0:T(1024)S(1)}, f32[2048]{0:T(1024)}, u32[]{:S(2)}) copy-start(f32[2048]{0:T(1024)} %param.30) | copy-start | bytes 24580
  80.6 2.2 %copy-start.1 = (f32[256,2048]{1,0:T(8,128)S(1)}, f32[256,2048]{1,0:T(8,128)}, u32[]{:S(2)}) copy-start(f32[256,2048]{1,0:T(8,128)} %reshape.265) | copy-start | bytes 6291460
  87.4 15.4 %all-to-all-start.1 = ((f32[128,2,24]{2,1,0:T(2,128)}), f32[128,2,24]{2,1,0:T(2,128)S(1)}, u32[]{:S(2)}, u32[]{:S(2)}) async-start(f32[128,2,24]{2,1,0:T(2,128)} %copy.77), calls=%async_computation.1 | async-start | bytes 262144 | tf_op jit(solution)/shard_map/all_to_all | solution.py:149
  92.9 4.0 %copy-start.12 = (f32[8]{0:T(128)S(1)}, f32[8]{0:T(128)}, u32[]{:S(2)}) copy-start(f32[8]{0:T(128)} %param.28) | copy-start | bytes 100
  102.9 5.3 %copy-start.7 = (bf16[2,512]{1,0:T(2,128)(2,1)}, bf16[2,512]{1,0:T(2,128)(2,1)S(1)}, u32[]{:S(2)}) copy-start(bf16[2,512]{1,0:T(2,128)(2,1)S(1)} %slice.111) | copy-start | bytes 6148
  105.8 2.4 %copy-start.10 = (f32[256]{0:T(256)S(1)}, f32[256]{0:T(256)}, u32[]{:S(2)}) copy-start(f32[256]{0:T(256)} %param.29) | copy-start | bytes 3076
  105.8 16.3 %copy-start.4 = (bf16[16,2048]{1,0:T(8,128)(2,1)S(1)}, bf16[16,2048]{1,0:T(8,128)(2,1)}, u32[]{:S(2)}) copy-start(bf16[16,2048]{1,0:T(8,128)(2,1)} %param.27) | copy-start | bytes 196612
  126.0 13.0 %copy-start.5 = (s32[256,6]{0,1:T(8,128)S(1)}, s32[256,6]{0,1:T(8,128)}, u32[]{:S(2)}) copy-start(s32[256,6]{0,1:T(8,128)} %param.32) | copy-start | bytes 18436
  131.0 20.9 %copy-start.3 = (bf16[2,2048]{1,0:T(2,128)(2,1)S(1)}, bf16[2,2048]{1,0:T(2,128)(2,1)}, u32[]{:S(2)}) copy-start(bf16[2,2048]{1,0:T(2,128)(2,1)} %param.20) | copy-start | bytes 24580
  131.0 21.0 %copy-start.8 = (f32[2048]{0:T(1024)S(1)}, f32[2048]{0:T(1024)}, u32[]{:S(2)}) copy-start(f32[2048]{0:T(1024)} %param.31) | copy-start | bytes 24580
  134.1 17.3 %all-to-all-start.4 = ((bf16[64,2,2048]{2,1,0:T(2,128)(2,1)}), bf16[64,2,2048]{2,1,0:T(2,128)(2,1)S(1)}, u32[]{:S(2)}, u32[]{:S(2)}) async-start(bf16[64,2,2048]{2,1,0:T(2,128)(2,1)} %reduce_sum.90), calls=%async_computation.4 | async-start | bytes 1048576 | tf_op jit(solution)/shard_map/all_to_all | solution.py:34
  153.9 24.7 %all-to-all-start.5 = ((bf16[128,2,2048]{2,1,0:T(2,128)(2,1)}), bf16[128,2,2048]{2,1,0:T(2,128)(2,1)S(1)}, u32[]{:S(2)}, u32[]{:S(2)}) async-start(bf16[128,2,2048]{2,1,0:T(2,128)(2,1)} %broadcast_select_fusion), calls=%async_computation.5 | async-start | bytes 2097152 | tf_op jit(solution)/shard_map/all_to_all | solution.py:182
  179.8 3.6 %copy-start.2 = (bf16[1,2048,512]{2,1,0:T(8,128)(2,1)S(1)}, bf16[1,2048,512]{2,1,0:T(8,128)(2,1)}, u32[]{:S(2)}) copy-start(bf16[1,2048,512]{2,1,0:T(8,128)(2,1)} %param.35) | copy-start | bytes 6291460
  184.5 6.0 %copy-start.9 = (f32[256,6]{0,1:T(8,128)S(1)}, f32[256,6]{0,1:T(8,128)}, u32[]{:S(2)}) copy-start(f32[256,6]{0,1:T(8,128)} %param.33) | copy-start | bytes 18436
  186.0 23.8 %all-to-all-start.6 = ((bf16[128,2,2048]{2,1,0:T(2,128)(2,1)}), bf16[128,2,2048]{2,1,0:T(2,128)(2,1)S(1)}, u32[]{:S(2)}, u32[]{:S(2)}) async-start(bf16[128,2,2048]{2,1,0:T(2,128)(2,1)} %reshape.260), calls=%async_computation.6 | async-start | bytes 2097152 | tf_op jit(solution)/shard_map/all_to_all | solution.py:186
Sparse Core Ops, SparseCore 0:
  10.8 67.1 all-gather.2
where the time goes:
time: 222 us; the launch traced here: 221 us
  waiting for transfers between devices  108 us (49%)
  starting transfers between devices  31.5 us (14%)
  local copies, waits for them, and re-layouts  20.6 us (9%)
  blocking collectives  18.6 us (8%)
  matrix products  17.3 us (8%)
  between operations  14.3 us (6%)
  other arithmetic  11.2 us (5%)
    all_gather x1, waiting for transfers between devices, on_device(): all_rows = lax.all_gather(hidden_in, EP, axis=0, tiled=True)  44.1 us
    all_to_all x1, waiting for transfers between devices, on_device(): lax.all_to_all(outgoing, EP, split_axis=0, concat_axis=0, tiled=True)  18.7 us
    all_to_all x1, waiting for transfers between devices, on_device(): lax.all_to_all(result.reshape(devices, tok_dev, model_width), EP, split_a...  16.4 us
    all_to_all x1, blocking collectives, on_device(): lax.all_to_all(attn_out, EP, split_axis=1, concat_axis=0, tiled=True)  13.7 us
    all_to_all x1, waiting for transfers between devices, summed_rows(): lax.all_to_all(nearer.astype(jnp.bfloat16), far, split_axis=0, concat_axi...  12.1 us
    all_to_all x1, starting transfers between devices, on_device(): lax.all_to_all(joined_rows, EP, split_axis=1, concat_axis=0, tiled=True)  11.5 us
    all_to_all x1, waiting for transfers between devices, on_device(): lax.all_to_all(joined_rows, EP, split_axis=1, concat_axis=0, tiled=True)  9.9 us
    all_to_all x1, waiting for transfers between devices, on_device(): lax.all_to_all(column_sums, EP, split_axis=0, concat_axis=1, tiled=True)  5.83 us
  transfers between devices with their start and end apart: 6, of which 6 were waited for; matrix products, arithmetic and copies ran while one was open for 5% of the time, Pallas kernels for 0%

commit v1 on v0

v1 whole, which is shorter than its diff:
```python
import jax
import jax.numpy as jnp
from jax import lax
from jax.sharding import Mesh
from jax.sharding import PartitionSpec as P

KV_HEADS = 2
HEAD_DIM = 128
EXP_CAP = 24
SLOTS = 32
AXES = ("z", "yh", "yl", "x", "c")
INNER = ("yl", "x", "c")
CHIPS = ("z", "yh", "yl", "x")

eps_norm = 1e-06
eps_head = 1e-05
theta_base = 500000.0
f32 = jnp.float32
bf16 = jnp.bfloat16


def exchange(value, axes):
    return lax.all_to_all(value, axes, split_axis=0, concat_axis=0, tiled=True)


def pair_swap(value):
    return lax.ppermute(value, "c", [(0, 1), (1, 0)])


def rms_scale(rows, gain, epsilon):
    rows = rows.astype(f32)
    return rows * lax.rsqrt(jnp.mean(rows * rows, axis=-1, keepdims=True) + epsilon) * gain


def rotate(vectors, positions):
    half_width = vectors.shape[-1] // 2
    inverse = theta_base ** (-jnp.arange(half_width, dtype=f32) / half_width)
    angles = positions.astype(f32)[..., None] * inverse
    cosine, sine = jnp.cos(angles), jnp.sin(angles)
    lower, upper = vectors[..., :half_width], vectors[..., half_width:]
    return jnp.concatenate([lower * cosine - upper * sine, lower * sine + upper * cosine], axis=-1)


def attend(queries, key_new, value_new, cache_keys, cache_values, lengths, lam_heads, head_gain):
    num_seqs, kv_heads, group_size = queries.shape[:3]
    head_dim = queries.shape[-1]
    cache_len = cache_keys.shape[1]
    cache_keys = cache_keys.reshape(num_seqs, cache_len, kv_heads, 2, head_dim)
    cache_values = cache_values.reshape(num_seqs, cache_len, kv_heads, -1)
    value_new = value_new.reshape(num_seqs, kv_heads, -1)
    score_scale = head_dim ** (-0.5)
    scores = (
        jnp.einsum("skgph,sckph->skgpc", queries, cache_keys, preferred_element_type=f32)
        * score_scale
    )
    self_score = (
        jnp.einsum("skgph,skph->skgp", queries, key_new, preferred_element_type=f32) * score_scale
    )
    live = (jnp.arange(cache_len)[None, :] < lengths[:, None])[:, None, None, None, :]
    peak = jnp.maximum(jnp.max(jnp.where(live, scores, -jnp.inf), axis=-1), self_score)
    weights = jnp.where(live, jnp.exp(scores - peak[..., None]), 0.0)
    self_weight = jnp.exp(self_score - peak)
    totals = jnp.sum(weights, axis=-1) + self_weight
    lam = lam_heads.reshape(kv_heads, group_size)[None]
    combined = (
        weights[:, :, :, 0] / totals[:, :, :, 0, None]
        - lam[..., None] * weights[:, :, :, 1] / totals[:, :, :, 1, None]
    ).astype(bf16)
    self_combined = (
        self_weight[..., 0] / totals[..., 0] - lam * self_weight[..., 1] / totals[..., 1]
    ).astype(bf16)
    head_out = jnp.einsum("skgc,sckv->skgv", combined, cache_values, preferred_element_type=f32)
    head_out = (
        head_out + self_combined.astype(f32)[..., None] * value_new.astype(f32)[:, :, None, :]
    )
    return rms_scale(head_out, head_gain, eps_head).astype(bf16).reshape(num_seqs, -1)


def on_device(
    hidden_in,
    lengths,
    key_cache,
    value_cache,
    query_w,
    key_w,
    value_w,
    out_w,
    lam_heads,
    head_gain,
    attn_gain,
    moe_gain,
    routing,
    route_weight,
    gate_w,
    up_w,
    down_w,
    shared_gate,
    shared_up,
    shared_down,
):
    n = lax.axis_size(AXES)
    device = lax.axis_index(AXES)
    core = lax.axis_index("c")
    chips = n // 2
    tok, width = hidden_in.shape
    tokens = tok * n
    inner = lax.axis_size(INNER)
    outer = n // inner
    span = width // outer
    cols = width // n

    normed = rms_scale(hidden_in, attn_gain, eps_norm).astype(bf16)
    slices = jnp.moveaxis(normed.reshape(tok, outer, span), 1, 0)
    slices = jnp.broadcast_to(slices[:, None], (outer, inner, tok, span)).reshape(n, tok, span)
    hidden_cols = hidden_in.reshape(tok, cols, n).transpose(2, 0, 1)
    arrived = exchange(jnp.concatenate([slices, hidden_cols], axis=2), AXES)
    rows = query_w.shape[0]
    blocks = [
        w.reshape(rows, inner, w.shape[1] // inner).transpose(1, 0, 2)
        for w in (query_w, key_w, value_w)
    ]
    qkv_w = exchange(jnp.concatenate(blocks, axis=2), INNER).reshape(span, -1)
    token_part = arrived[:, :, :span].reshape(tokens, span)
    hidden_part = arrived[:, :, span:].reshape(tokens, cols)

    ow = out_w.reshape(rows * cols, n).T.reshape(chips, 1, 2 * rows * cols)
    ow = jnp.broadcast_to(ow, (chips, 2, 2 * rows * cols)).reshape(n, -1, 128)
    ow = exchange(ow, AXES)
    ow = lax.dynamic_slice_in_dim(ow, core * chips, chips, 0)
    ow = ow.reshape(chips, 2, rows, cols).transpose(0, 2, 1, 3).reshape(chips * rows, 2 * cols)

    sums = jnp.dot(token_part, qkv_w, preferred_element_type=f32)
    sums = exchange(sums.reshape(n, tok, -1), AXES)
    sums = sums.reshape(outer, inner, tok, -1).sum(axis=0)
    q_part = query_w.shape[1] // inner
    k_part = key_w.shape[1] // inner
    q_raw = sums[:, :, :q_part].transpose(1, 0, 2)
    k_raw = sums[:, :, q_part : q_part + k_part].transpose(1, 0, 2)
    value_new = sums[:, :, q_part + k_part :].transpose(1, 0, 2).reshape(tok, -1).astype(bf16)
    queries = rotate(
        q_raw.reshape(tok, KV_HEADS, -1, 2, HEAD_DIM), lengths[:, None, None, None]
    ).astype(bf16)
    key_new = rotate(
        k_raw.reshape(tok, KV_HEADS, 2, HEAD_DIM), lengths[:, None, None]
    ).astype(bf16)
    attn_out = attend(
        queries, key_new, value_new, key_cache, value_cache, lengths, lam_heads, head_gain
    )

    half = width // 2
    pieces = jnp.moveaxis(attn_out.reshape(tok, 2, half), 1, 0)
    pieces = jnp.broadcast_to(pieces[None], (chips, 2, tok, half)).reshape(n, tok, half)
    pieces = exchange(pieces, AXES).reshape(tokens, half)
    partial = jnp.dot(pieces, ow, preferred_element_type=f32)
    mine = jnp.where(core == 0, partial[:, :cols], partial[:, cols:])
    theirs = jnp.where(core == 0, partial[:, cols:], partial[:, :cols])
    attn_proj = (mine + pair_swap(theirs)).astype(bf16)
    mixed_cols = (hidden_part.astype(f32) + attn_proj.astype(f32)).astype(bf16)

    ids = jnp.arange(n, dtype=jnp.int32)
    match = routing[:, :, None] == ids
    named = jnp.any(match, axis=1)
    weight_of = jnp.sum(jnp.where(match, route_weight[:, :, None], 0.0), axis=1)
    t_ids = jnp.arange(tokens, dtype=jnp.int32)
    below = (t_ids[:, None] >= t_ids[None, :]).astype(bf16)
    slot = jnp.dot(below, named.astype(bf16), preferred_element_type=f32).astype(jnp.int32) - 1
    slot = jnp.where(named, slot, -1)
    s_ids = jnp.arange(SLOTS, dtype=jnp.int32)
    pick = slot.T[:, None, :] == s_ids[None, :, None]
    own = t_ids[None, None, :] == (ids[:, None] * tok + s_ids[None, :] - EXP_CAP)[:, :, None]
    last = (s_ids >= EXP_CAP) & (s_ids < EXP_CAP + tok)
    pick = jnp.where(last[None, :, None], own, pick & (s_ids < EXP_CAP)[None, :, None])
    pick = pick.astype(bf16)

    chosen = jnp.dot(pick.reshape(n * SLOTS, tokens), mixed_cols, preferred_element_type=f32)
    chosen = chosen.astype(bf16).reshape(n, SLOTS * cols // 128, 128)
    chosen = exchange(chosen, AXES).reshape(n, SLOTS, cols)
    mixed = chosen.transpose(1, 2, 0).reshape(SLOTS, width)
    moe_in = rms_scale(mixed, moe_gain, eps_norm).astype(bf16)
    hidden = (
        jax.nn.silu(jnp.dot(moe_in, gate_w[0], preferred_element_type=f32))
        * jnp.dot(moe_in, up_w[0], preferred_element_type=f32)
    ).astype(bf16)
    result = jnp.dot(hidden, down_w[0], preferred_element_type=f32).astype(bf16)

    kept = lax.dynamic_slice_in_dim(result, core * half, half, 1)
    given = lax.dynamic_slice_in_dim(result, (1 - core) * half, half, 1)
    given = pair_swap(given[:EXP_CAP])
    stacked = jnp.concatenate([kept[:EXP_CAP], given], axis=0)

    def spread(expert):
        sl = lax.dynamic_slice_in_dim(slot, expert, 1, 1)
        w = lax.dynamic_slice_in_dim(weight_of, expert, 1, 1)
        return jnp.where(sl == s_ids[None, :EXP_CAP], w, 0.0)

    table = jnp.concatenate([spread(device), spread(device + 1 - 2 * core)], axis=1)
    high = table.astype(bf16)
    low = (table - high.astype(f32)).astype(bf16)
    summed = jnp.dot(
        jnp.concatenate([high, low], axis=1),
        jnp.concatenate([stacked, stacked], axis=0),
        preferred_element_type=f32,
    ).astype(bf16)
    back = exchange(summed.reshape(n, tok, half), AXES)
    routed = jnp.sum(back.reshape(chips, 2, tok, half).astype(f32), axis=0)
    routed = jnp.moveaxis(routed, 0, 1).reshape(tok, width)

    after_mixer = mixed[EXP_CAP : EXP_CAP + tok]
    own_in = moe_in[EXP_CAP : EXP_CAP + tok]
    shared_hidden = (
        jax.nn.silu(jnp.dot(own_in, shared_gate, preferred_element_type=f32))
        * jnp.dot(own_in, shared_up, preferred_element_type=f32)
    ).astype(bf16)
    shared_out = jnp.dot(shared_hidden, shared_down, preferred_element_type=f32)
    layer_out = (after_mixer.astype(f32) + routed + shared_out).astype(bf16)
    return (layer_out, key_new.reshape(tok, -1), value_new)


def solution(mesh):
    torus = Mesh(mesh.devices.reshape(4, 2, 2, 4, 2), AXES)
    split = P(AXES)
    return jax.shard_map(
        on_device,
        mesh=torus,
        in_specs=(split,) * 8 + (P(),) * 6 + (split,) * 3 + (P(),) * 3,
        out_specs=(split, split, split),
        check_vma=False,
    )
```

time: 222 us -> 149 us (0.67)
  waiting for transfers between devices: 108 us -> 50.9 us
  blocking collectives: 18.6 us -> 0 us
  between operations: 14.3 us -> 1.22 us
  starting transfers between devices: 31.5 us -> 44.3 us
    all_gather x1 -> x0, waiting for transfers between devices: 44.1 us -> none  [on_device(): all_rows = lax.all_gather(hidden_in, EP, axis=0, tiled=True)]
    all_to_all x2 -> x0, blocking collectives: 18.6 us -> none  [the longest x1 13.7 us: on_device(): lax.all_to_all(attn_out, EP, split_axis=1, concat_axis=0, tiled=True)]
    all_to_all x5 -> x7, waiting for transfers between devices: 63 us -> 50 us  [exchange(): return lax.all_to_all(value, axes, split_axis=0, concat_axis=0, tiled=True)]
    all_to_all x5 -> x7, starting transfers between devices: 31.5 us -> 42.8 us  [exchange(): return lax.all_to_all(value, axes, split_axis=0, concat_axis=0, tiled=True)]
    reduce_sum x7 -> x4, other arithmetic: 6.87 us -> 2.31 us  [the longest x2 1.3 us: rms_scale(): jnp.mean(rows * rows, axis=-1, keepdims=True) + epsilon]
    another operation x3 -> x1, local copies, waits for them, and re-layouts: 3.58 us -> 0.01 us  [on_device(): pieces = jnp.moveaxis(attn_out.reshape(tok, 2, half), 1, 0)]
    reshape x4 -> x10, local copies, waits for them, and re-layouts: 2.77 us -> 5.92 us  [the longest x2 1.65 us: on_device(): w.reshape(rows, inner, w.shape[1] // inner).transpose(1, 0, 2)]
    and x0 -> x2, other arithmetic: none -> 2.65 us  [the longest x1 2.65 us: on_device(): pick & (s_ids < EXP_CAP)[None, :, None]]
  transfers between devices with their start and end apart: 6 -> 9, of which waited for: 6 -> 7; matrix products, arithmetic and copies ran while one was open for 5% -> 20% of each run, Pallas kernels for 0% -> 0%
where the time goes in v1:
time: 149 us; the launch traced here: 147 us
  waiting for transfers between devices  50.9 us (34%)
  starting transfers between devices  44.3 us (30%)
  local copies, waits for them, and re-layouts  20.4 us (14%)
  matrix products  18.7 us (13%)
  other arithmetic  11.9 us (8%)
    all_to_all x7, waiting for transfers between devices, exchange(): return lax.all_to_all(value, axes, split_axis=0, concat_axis=0, tiled=True)  50 us
    all_to_all x7, starting transfers between devices, exchange(): return lax.all_to_all(value, axes, split_axis=0, concat_axis=0, tiled=True)  42.8 us
    reshape x1, local copies, waits for them, and re-layouts, attend(): cache_keys = cache_keys.reshape(num_seqs, cache_len, kv_heads, 2, head_dim)  4.01 us
    dot_general x1, matrix products, on_device(): shared_out = jnp.dot(shared_hidden, shared_down, preferred_element_type=f32)  3.59 us
  transfers between devices with their start and end apart: 9, of which 7 were waited for; matrix products, arithmetic and copies ran while one was open for 20% of the time, Pallas kernels for 0%

profile of v1, /device:TPU:1, one launch (start us, length us, event | category | flops | bytes accessed | tf_op | source)
XLA Modules:
  0.0 147.4 jit_solution(7855577844626662912)
XLA Ops:
  4.3 11.5 %all-to-all-start = ((bf16[128,2,272]{2,1,0:T(2,128)(2,1)}), bf16[128,2,272]{2,1,0:T(2,128)(2,1)S(1)}, u32[]{:S(2)}, u32[]{:S(2)}) async-start(bf16[128,2,272]{2,1,0:T(2,128)(2,1)} %pad_maximum_fusion), calls=%async_computation | async-start | bytes 393216 | tf_op jit(solution)/shard_map/all_to_all | solution.py:23
  21.7 4.0 %reshape.354 = bf16[2,1024,2,2,128]{4,3,2,1,0:T(2,128)(2,1)} reshape(bf16[2,1024,512]{2,1,0:T(8,128)(2,1)} %param.22) | data formatting | bytes 4194304 | tf_op jit(solution)/shard_map/reshape | solution.py:48
  27.5 5.7 %all-to-all-start.1 = ((bf16[16,16,192]{2,1,0:T(8,128)(2,1)}), bf16[16,16,192]{2,1,0:T(8,128)(2,1)S(1)}, u32[]{:S(2)}, u32[]{:S(2)}) async-start(bf16[16,16,192]{2,1,0:T(8,128)(2,1)} %pad_maximum_fusion.1), calls=%async_computation.1 | async-start | bytes 262144 | tf_op jit(solution)/shard_map/all_to_all | solution.py:23
  33.9 5.4 %all-to-all-done.1 = bf16[16,16,192]{2,1,0:T(8,128)(2,1)S(1)} async-done(((bf16[16,16,192]{2,1,0:T(8,128)(2,1)}), bf16[16,16,192]{2,1,0:T(8,128)(2,1)S(1)}, u32[]{:S(2)}, u32[]{:S(2)}) %all-to-all-start.1) | async-done | bytes 98336 | tf_op jit(solution)/shard_map/all_to_all | solution.py:23
  40.4 7.7 %all-to-all-start.2 = ((f32[128,2,192]{2,1,0:T(2,128)}), f32[128,2,192]{2,1,0:T(2,128)S(1)}, u32[]{:S(2)}, u32[]{:S(2)}) async-start(f32[128,2,192]{2,1,0:T(2,128)} %copy.108), calls=%async_computation.2 | async-start | bytes 524288 | tf_op jit(solution)/shard_map/all_to_all | solution.py:23
  48.2 11.0 %all-to-all-done.2 = f32[128,2,192]{2,1,0:T(2,128)S(1)} async-done(((f32[128,2,192]{2,1,0:T(2,128)}), f32[128,2,192]{2,1,0:T(2,128)S(1)}, u32[]{:S(2)}, u32[]{:S(2)}) %all-to-all-start.2) | async-done | bytes 196640 | tf_op jit(solution)/shard_map/all_to_all | solution.py:23
  59.1 4.4 %all-to-all-start.4 = ((bf16[128,4,128]{2,1,0:T(4,128)(2,1)}), bf16[128,4,128]{2,1,0:T(4,128)(2,1)S(1)}, u32[]{:S(2)}, u32[]{:S(2)}) async-start(bf16[128,4,128]{2,1,0:T(4,128)(2,1)} %reshape.360), calls=%async_computation.4 | async-start | bytes 262144 | tf_op jit(solution)/shard_map/all_to_all | solution.py:23
  64.4 2.4 %select_reduce_fusion.1 = (f32[2,2,4,2]{2,3,1,0:T(2,128)S(1)}, f32[2,2,4,2,1024]{4,2,3,1,0:T(4,128)S(1)}) fusion(pred[2,1024]{1,0:T(4,128)(4,1)S(1)} %iota_compare_fusion.4, bf16[2,1024,2,2,128]{4,3,2,1,0:T(2,128)(2,1)} %reshape.354, bf16[2,2,4,2,64]{4,2,3,1,0:T(4,128)(2,1)S(1)} %get-tuple-element.14, bf16[2,2,4,2,64]{4,2,3,1,0:T(4,128)(2,1)S(1)} %get-tuple-element.13), kind=kOutput, calls=%fused_computation.55 | convolution fusion | flops 8503264 | bytes 2238592 | tf_op jit(solution)/shard_map/skgph,sckph->skgpc/dot_general | solution.py:53
  67.1 2.1 %multiply_reduce_fusion.1 = (f32[2,2,4]{2,1,0:T(2,128)S(1)}, f32[2,2,4,256]{3,2,1,0:T(4,128)S(1)}) fusion(f32[2,2,256]{2,1,0:T(2,128)S(1)} %reshape.369, f32[2,2,4]{2,1,0:T(2,128)S(1)} %bitcast.189, bf16[2,128,2,8,256]{4,3,2,1,0:T(8,128)(2,1)} %bitcast.193, f32[2,2,4,2,1024]{4,2,3,1,0:T(4,128)S(1)} %get-tuple-element.8, f32[2,2,4]{2,1,0:T(2,128)S(1)} %bitcast.190, ...), kind=kOutput, calls=%fused_computation.98 | convolution fusion | flops 8486896 | bytes 2248992 | tf_op jit(solution)/shard_map/skgc,sckv->skgv/dot_general | solution.py:72
  69.4 4.2 %all-to-all-done.4 = bf16[128,4,128]{2,1,0:T(4,128)(2,1)S(1)} async-done(((bf16[128,4,128]{2,1,0:T(4,128)(2,1)}), bf16[128,4,128]{2,1,0:T(4,128)(2,1)S(1)}, u32[]{:S(2)}, u32[]{:S(2)}) %all-to-all-start.4) | async-done | bytes 131104 | tf_op jit(solution)/shard_map/all_to_all | solution.py:23
  74.7 5.6 %all-to-all-start.3 = ((bf16[128,2,1024]{2,1,0:T(2,128)(2,1)}), bf16[128,2,1024]{2,1,0:T(2,128)(2,1)S(1)}, u32[]{:S(2)}, u32[]{:S(2)}) async-start(bf16[128,2,1024]{2,1,0:T(2,128)(2,1)} %bitcast.30), calls=%async_computation.3 | async-start | bytes 1048576 | tf_op jit(solution)/shard_map/all_to_all | solution.py:23
  82.5 1.2 copy.118
  84.5 9.4 %all-to-all-done.3 = bf16[128,2,1024]{2,1,0:T(2,128)(2,1)S(1)} async-done(((bf16[128,2,1024]{2,1,0:T(2,128)(2,1)}), bf16[128,2,1024]{2,1,0:T(2,128)(2,1)S(1)}, u32[]{:S(2)}, u32[]{:S(2)}) %all-to-all-start.3) | async-done | bytes 524320 | tf_op jit(solution)/shard_map/all_to_all | solution.py:23
  96.2 2.6 %fusion.2 = pred[4096,256]{1,0:T(32,128)(4,1)S(1)} fusion(s32[4096]{0:T(1024)S(1)} %add.127, s32[128,256]{1,0:T(8,128)} %bitcast.174, pred[4096]{0:T(1024)(128)(4,1)S(1)} %and.27), kind=kLoop, calls=%fused_computation.4 | loop fusion | flops 2097152 | bytes 1200128 | tf_op jit(solution)/shard_map/and | solution.py:172
  99.3 2.8 %convolution_convert_fusion = bf16[4096,16]{0,1:T(8,128)(2,1)S(1)} fusion(pred[4096,256]{1,0:T(32,128)(4,1)S(1)} %fusion.2, s32[4096]{0:T(1024)} %add_add_fusion, pred[4096]{0:T(1024)(128)(4,1)S(1)} %broadcast_in_dim.75, f32[256,16]{0,1:T(8,128)S(1)} %copy.119, f32[256,16]{0,1:T(8,128)S(1)} %collective-permute-done, f32[256,32]{0,1:T(8,128)} %copy-done.2, ...), kind=kOutput, calls=%fused_computation | convolution fusion | flops 35741696 | bytes 1265665 | tf_op jit(solution)/shard_map/dot_general | solution.py:175
  102.6 1.3 reshape.363
  104.0 3.8 %all-to-all-start.5 = ((bf16[128,4,128]{2,1,0:T(4,128)(2,1)}), bf16[128,4,128]{2,1,0:T(4,128)(2,1)S(1)}, u32[]{:S(2)}, u32[]{:S(2)}) async-start(bf16[128,4,128]{2,1,0:T(4,128)(2,1)} %reshape.363), calls=%async_computation.5 | async-start | bytes 262144 | tf_op jit(solution)/shard_map/all_to_all | solution.py:23
  107.8 9.9 %all-to-all-done.5 = bf16[128,4,128]{2,1,0:T(4,128)(2,1)S(1)} async-done(((bf16[128,4,128]{2,1,0:T(4,128)(2,1)}), bf16[128,4,128]{2,1,0:T(4,128)(2,1)S(1)}, u32[]{:S(2)}, u32[]{:S(2)}) %all-to-all-start.5) | async-done | bytes 131104 | tf_op jit(solution)/shard_map/all_to_all | solution.py:23
  118.3 2.0 %fusion.10 = f32[32,512]{1,0:T(8,128)S(1)} fusion(bf16[1,2048,512]{2,1,0:T(8,128)(2,1)} %param.34, bf16[4,8,16,128]{3,2,1,0:T(8,128)(2,1)S(1)} %bitcast.163), kind=kOutput, calls=%fused_computation.14 | convolution fusion | flops 67108864 | bytes 2293760 | tf_op jit(solution)/shard_map/dot_general | solution.py:181
  120.4 2.5 %convolution_convert_fusion.1 = bf16[32,2048]{1,0:T(8,128)(2,1)S(1)} fusion(bf16[1,512,2048]{2,1,0:T(8,128)(2,1)S(1)} %copy-done, bf16[1,2048,512]{2,1,0:T(8,128)(2,1)} %param.35, bf16[4,8,16,128]{3,2,1,0:T(8,128)(2,1)S(1)} %bitcast.164, f32[32,512]{1,0:T(8,128)S(1)} %fusion.10), kind=kOutput, calls=%fused_computation.5 | convolution fusion | flops 134381568 | bytes 4521984 | tf_op jit(solution)/shard_map/dot_general | solution.py:184
  125.7 4.1 %all-to-all-start.6 = ((bf16[128,2,1024]{2,1,0:T(2,128)(2,1)}), bf16[128,2,1024]{2,1,0:T(2,128)(2,1)S(1)}, u32[]{:S(2)}, u32[]{:S(2)}) async-start(bf16[128,2,1024]{2,1,0:T(2,128)(2,1)} %reshape.365), calls=%async_computation.6 | async-start | bytes 1048576 | tf_op jit(solution)/shard_map/all_to_all | solution.py:23
  131.3 2.0 %fusion.87 = f32[2,512]{1,0:T(2,128)S(1)} fusion(bf16[2048,512]{1,0:T(8,128)(2,1)} %param.37, f32[32,2048]{1,0:T(8,128)S(1)} %bitcast.166, f32[2]{0:T(128)S(1)} %slice.115, f32[2048]{0:T(1024)S(1)} %copy-done.3), kind=kOutput, calls=%fused_computation.144 | convolution fusion | flops 4206592 | bytes 2126336 | tf_op jit(solution)/shard_map/dot_general | solution.py:211
  133.3 10.1 %all-to-all-done.6 = bf16[128,2,1024]{2,1,0:T(2,128)(2,1)S(1)} async-done(((bf16[128,2,1024]{2,1,0:T(2,128)(2,1)}), bf16[128,2,1024]{2,1,0:T(2,128)(2,1)S(1)}, u32[]{:S(2)}, u32[]{:S(2)}) %all-to-all-start.6) | async-done | bytes 524320 | tf_op jit(solution)/shard_map/all_to_all | solution.py:23
  143.8 3.6 %fusion.3 = bf16[2,2048]{1,0:T(2,128)(2,1)} fusion(bf16[512,2048]{1,0:T(8,128)(2,1)} %param.39, bf16[2048,512]{1,0:T(8,128)(2,1)} %param.38, f32[2,2048]{1,0:T(2,128)S(1)} %bitcast.179, f32[1,2,16,128]{3,2,1,0:T(8,128)S(1)} %convert_bitcast_fusion, f32[2,512]{1,0:T(2,128)S(1)} %fusion.87, f32[32,2048]{1,0:T(8,128)S(1)} %bitcast.167, f32[2]{0:T(128)S(1)} %slice.115, ...), kind=kOutput, calls=%fused_computation.7 | convolution fusion | flops 8419328 | bytes 4264448 | tf_op jit(solution)/shard_map/dot_general | solution.py:214
  (134 shorter events, 26.8 us)
Async XLA Ops:
  0.6 119.8 %copy-start = (bf16[1,512,2048]{2,1,0:T(8,128)(2,1)S(1)}, bf16[1,512,2048]{2,1,0:T(8,128)(2,1)}, u32[]{:S(2)}) copy-start(bf16[1,512,2048]{2,1,0:T(8,128)(2,1)} %param.36) | copy-start | bytes 6291460
  4.3 23.3 %all-to-all-start = ((bf16[128,2,272]{2,1,0:T(2,128)(2,1)}), bf16[128,2,272]{2,1,0:T(2,128)(2,1)S(1)}, u32[]{:S(2)}, u32[]{:S(2)}) async-start(bf16[128,2,272]{2,1,0:T(2,128)(2,1)} %pad_maximum_fusion), calls=%async_computation | async-start | bytes 393216 | tf_op jit(solution)/shard_map/all_to_all | solution.py:23
  20.4 5.3 %copy-start.1 = (s32[256,128]{0,1:T(8,128)}, s32[256,128]{0,1:T(8,128)S(1)}, u32[]{:S(2)}) copy-start(s32[256,128]{0,1:T(8,128)S(1)} %fusion.17) | copy-start | bytes 393220
  21.7 4.0 %copy-start.16 = (f32[8]{0:T(128)S(1)}, f32[8]{0:T(128)}, u32[]{:S(2)}) copy-start(f32[8]{0:T(128)} %param.28) | copy-start | bytes 100
  21.7 4.1 %copy-start.6 = (bf16[16,2048]{1,0:T(8,128)(2,1)S(1)}, bf16[16,2048]{1,0:T(8,128)(2,1)}, u32[]{:S(2)}) copy-start(bf16[16,2048]{1,0:T(8,128)(2,1)} %param.27) | copy-start | bytes 196612
  27.5 11.8 %all-to-all-start.1 = ((bf16[16,16,192]{2,1,0:T(8,128)(2,1)}), bf16[16,16,192]{2,1,0:T(8,128)(2,1)S(1)}, u32[]{:S(2)}, u32[]{:S(2)}) async-start(bf16[16,16,192]{2,1,0:T(8,128)(2,1)} %pad_maximum_fusion.1), calls=%async_computation.1 | async-start | bytes 262144 | tf_op jit(solution)/shard_map/all_to_all | solution.py:23
  40.4 18.8 %all-to-all-start.2 = ((f32[128,2,192]{2,1,0:T(2,128)}), f32[128,2,192]{2,1,0:T(2,128)S(1)}, u32[]{:S(2)}, u32[]{:S(2)}) async-start(f32[128,2,192]{2,1,0:T(2,128)} %copy.108), calls=%async_computation.2 | async-start | bytes 524288 | tf_op jit(solution)/shard_map/all_to_all | solution.py:23
  59.1 14.4 %all-to-all-start.4 = ((bf16[128,4,128]{2,1,0:T(4,128)(2,1)}), bf16[128,4,128]{2,1,0:T(4,128)(2,1)S(1)}, u32[]{:S(2)}, u32[]{:S(2)}) async-start(bf16[128,4,128]{2,1,0:T(4,128)(2,1)} %reshape.360), calls=%async_computation.4 | async-start | bytes 262144 | tf_op jit(solution)/shard_map/all_to_all | solution.py:23
  64.0 5.2 %copy-start.8 = (bf16[2,2,2,64]{3,2,1,0:T(2,128)(2,1)}, bf16[2,2,2,64]{3,2,1,0:T(2,128)(2,1)S(1)}, u32[]{:S(2)}) copy-start(bf16[2,2,2,64]{3,2,1,0:T(2,128)(2,1)S(1)} %get-tuple-element.17) | copy-start | bytes 3076
  64.1 5.2 %copy-start.10 = (bf16[2,2,2,64]{3,2,1,0:T(2,128)(2,1)}, bf16[2,2,2,64]{3,2,1,0:T(2,128)(2,1)S(1)}, u32[]{:S(2)}) copy-start(bf16[2,2,2,64]{3,2,1,0:T(2,128)(2,1)S(1)} %get-tuple-element.18) | copy-start | bytes 3076
  67.0 7.7 %copy-start.4 = (bf16[16,2,32]{2,0,1:T(8,128)(2,1)}, bf16[16,2,32]{2,0,1:T(8,128)(2,1)S(1)}, u32[]{:S(2)}) copy-start(bf16[16,2,32]{2,0,1:T(8,128)(2,1)S(1)} %copy.187) | copy-start | bytes 6148
  67.1 13.4 %copy-start.7 = (s32[256,6]{0,1:T(8,128)S(1)}, s32[256,6]{0,1:T(8,128)}, u32[]{:S(2)}) copy-start(s32[256,6]{0,1:T(8,128)} %param.32) | copy-start | bytes 18436
  67.1 13.4 %copy-start.12 = (f32[256,6]{0,1:T(8,128)S(1)}, f32[256,6]{0,1:T(8,128)}, u32[]{:S(2)}) copy-start(f32[256,6]{0,1:T(8,128)} %param.33) | copy-start | bytes 18436
  74.7 19.2 %all-to-all-start.3 = ((bf16[128,2,1024]{2,1,0:T(2,128)(2,1)}), bf16[128,2,1024]{2,1,0:T(2,128)(2,1)S(1)}, u32[]{:S(2)}, u32[]{:S(2)}) async-start(bf16[128,2,1024]{2,1,0:T(2,128)(2,1)} %bitcast.30), calls=%async_computation.3 | async-start | bytes 1048576 | tf_op jit(solution)/shard_map/all_to_all | solution.py:23
  94.3 4.9 %collective-permute-start = (f32[256,16]{0,1:T(8,128)S(1)}, f32[256,16]{0,1:T(8,128)S(1)}, u32[]{:S(2)}, u32[]{:S(2)}) collective-permute-start(f32[256,16]{0,1:T(8,128)S(1)} %slice_select_fusion), channel_id=1, source_target_pairs={{0,1},{1,0},{2,3},{3,2},{4,5},{5,4},{6,7},{7,6},{8,9},{9,8},{10,11... | collective-permute-start | bytes 49160 | tf_op jit(solution)/shard_map/ppermute | solution.py:27
  102.1 5.6 %copy-start.13 = (s32[256,1]{0,1:T(1,128)S(1)}, s32[256,1]{0,1:T(1,128)}, u32[]{:S(2)}) copy-start(s32[256,1]{0,1:T(1,128)} %get-tuple-element.9) | copy-start | bytes 3076
  102.1 5.6 %copy-start.14 = (s32[256,1]{0,1:T(1,128)S(1)}, s32[256,1]{0,1:T(1,128)}, u32[]{:S(2)}) copy-start(s32[256,1]{0,1:T(1,128)} %get-tuple-element.10) | copy-start | bytes 3076
  102.1 16.1 %copy-start.3 = (f32[2048]{0:T(1024)S(1)}, f32[2048]{0:T(1024)}, u32[]{:S(2)}) copy-start(f32[2048]{0:T(1024)} %param.31) | copy-start | bytes 24580
  104.0 13.8 %all-to-all-start.5 = ((bf16[128,4,128]{2,1,0:T(4,128)(2,1)}), bf16[128,4,128]{2,1,0:T(4,128)(2,1)S(1)}, u32[]{:S(2)}, u32[]{:S(2)}) async-start(bf16[128,4,128]{2,1,0:T(4,128)(2,1)} %reshape.363), calls=%async_computation.5 | async-start | bytes 262144 | tf_op jit(solution)/shard_map/all_to_all | solution.py:23
  122.9 6.9 %copy-start.9 = (bf16[2,2,2,64]{3,2,1,0:T(2,128)(2,1)S(1)}, bf16[2,2,2,64]{3,2,1,0:T(2,128)(2,1)}, u32[]{:S(2)}) copy-start(bf16[2,2,2,64]{3,2,1,0:T(2,128)(2,1)} %copy-done.8) | copy-start | bytes 3076
  122.9 6.9 %copy-start.11 = (bf16[2,2,2,64]{3,2,1,0:T(2,128)(2,1)S(1)}, bf16[2,2,2,64]{3,2,1,0:T(2,128)(2,1)}, u32[]{:S(2)}) copy-start(bf16[2,2,2,64]{3,2,1,0:T(2,128)(2,1)} %copy-done.10) | copy-start | bytes 3076
  122.9 7.0 %copy-start.5 = (bf16[16,2,32]{2,0,1:T(8,128)(2,1)S(1)}, bf16[16,2,32]{2,0,1:T(8,128)(2,1)}, u32[]{:S(2)}) copy-start(bf16[16,2,32]{2,0,1:T(8,128)(2,1)} %copy-done.4) | copy-start | bytes 6148
  123.0 1.4 collective-permute-start.1
  125.7 17.7 %all-to-all-start.6 = ((bf16[128,2,1024]{2,1,0:T(2,128)(2,1)}), bf16[128,2,1024]{2,1,0:T(2,128)(2,1)S(1)}, u32[]{:S(2)}, u32[]{:S(2)}) async-start(bf16[128,2,1024]{2,1,0:T(2,128)(2,1)} %reshape.365), calls=%async_computation.6 | async-start | bytes 1048576 | tf_op jit(solution)/shard_map/all_to_all | solution.py:23
  (2 other events, 4.5 us)
